TPU v7x, 256 devices: a whole 4x4x8 slice. The times are simulated.
256 devices in a mesh: ep: 16 (over y, x), tp: 16 (over z, core).
Axes of the slice: x: 4, y: 4, z: 8, core: 2. Of those that a mesh axis runs over, the one named last changes fastest.
Arguments:
- mix_tokens: bfloat16 [4096, 4096], P('ep'), may hold values from -6 to 6
- mix_gain: float32 [4096], replicated, may hold values from 0.1 to 1.9
- value_weight: bfloat16 [4096, 2048], P(None, 'tp'), may hold values from -0.09375 to 0.09375
- inner_weight: bfloat16 [4096, 2048], P(None, 'tp'), may hold values from -0.09375 to 0.09375
- outer_weight: bfloat16 [4096, 2048], P(None, 'tp'), may hold values from -0.09375 to 0.09375
- conv_taps: float32 [3, 2048], P(None, 'tp'), may hold values from -3 to 3
- mix_weight: bfloat16 [2048, 4096], P('tp'), may hold values from -0.125 to 0.125
- moe_tokens: bfloat16 [4096, 4096], P('ep'), may hold values from -6 to 6
- moe_gain: float32 [4096], replicated, may hold values from 0.1 to 1.9
- router_group: bfloat16 [4096, 4], replicated, may hold values from -0.09375 to 0.09375
- router_expert: bfloat16 [4096, 16], replicated, may hold values from -0.09375 to 0.09375
- expert_routes: int32 [4096, 2], P('ep'), may hold values from 0 to 15, as said below
- gate_weight: bfloat16 [16, 4096, 2048], P('ep', None, 'tp'), may hold values from -0.09375 to 0.09375
- up_weight: bfloat16 [16, 4096, 2048], P('ep', None, 'tp'), may hold values from -0.09375 to 0.09375
- down_weight: bfloat16 [16, 2048, 4096], P('ep', 'tp'), may hold values from -0.5 to 0.5
Outputs:
- mixer_out: bfloat16 [4096, 4096], P(('ep', 'tp'))
- expert_out: bfloat16 [4096, 4096], P(('ep', 'tp'))
Inputs may be any that keep to these rules, and one draw needn't show every extreme that they name: `expert_routes`: the two experts of a row are different and lie in one group of 4 consecutive expert numbers. In each aligned block of 16 rows no expert is named more than 4 times, and in every draw some experts are named exactly 4 times in every block.
All inputs are finite; a program needn't handle non-finite values.
Results may differ from a plain program's by a relative error of at most 0.0076.
Values may be sent and summed in bfloat16 or wider, within the bound.
No kernel may reach another device: no remote copies, remote signals or barrier semaphores. Data moves between devices by JAX's collectives and lax.ppermute only.
A program may use at most 128 MiB of HBM per device.

v0:
```python
import jax
import jax.numpy as jnp
from jax import lax
from jax.sharding import PartitionSpec as P

TAPS = 3
EXPERTS = 16
GROUPS = 4
TOPK = 2
MOE_SHARE = 16
EPG = 4
CAP = 4


def from_behind(value, axis, steps):
    count = lax.axis_size(axis)
    initial, last = (max(0, -steps), min(count, count - steps))
    return lax.ppermute(value, axis, [(source, source + steps) for source in range(initial, last)])


def rms_rows(inputs, gain_vec):
    values = inputs.astype(jnp.float32)
    inverse = lax.rsqrt(jnp.mean(values * values, axis=-1, keepdims=True) + 1e-06)
    return (values * inverse * gain_vec).astype(jnp.bfloat16)


def route_weights(normed, routes, router_group, router_expert):
    group_logit = jnp.dot(normed, router_group, preferred_element_type=jnp.float32)
    expert_logit = jnp.dot(normed, router_expert, preferred_element_type=jnp.float32)
    group_exp = jnp.exp(group_logit)
    group_id = routes[:, 0] // EPG
    group_pick = (group_id[:, None] == jnp.arange(GROUPS, dtype=jnp.int32)[None, :]).astype(
        jnp.float32
    )
    group_gate = jnp.sum(group_exp * group_pick, axis=1) / jnp.sum(group_exp, axis=1)
    expert_pick = (
        routes[:, :, None] == jnp.arange(EXPERTS, dtype=jnp.int32)[None, None, :]
    ).astype(jnp.float32)
    chosen = jnp.exp(jnp.sum(expert_logit[:, None, :] * expert_pick, axis=2))
    return group_gate[:, None] * chosen / jnp.sum(chosen, axis=1, keepdims=True)


def block_ranks(routes):
    blocks = routes.shape[0]
    entries = routes.reshape(blocks, MOE_SHARE * TOPK)
    one_hot = (entries[:, :, None] == jnp.arange(EXPERTS, dtype=jnp.int32)[None, None, :]).astype(
        jnp.int32
    )
    before = jnp.cumsum(one_hot, axis=1) - one_hot
    return jnp.sum(before * one_hot, axis=2).reshape(routes.shape)


def dispatch_rows(normed, routes):
    slot_ids = routes * CAP + block_ranks(routes)
    targets = jnp.arange(EXPERTS * CAP, dtype=jnp.int32)
    select = (slot_ids[:, None, :, :] == targets[None, :, None, None]).astype(jnp.int32)
    select = jnp.sum(select, axis=3).astype(jnp.bfloat16)
    placed = jnp.einsum("bcs,bsd->bcd", select, normed, preferred_element_type=jnp.float32)
    return placed.astype(jnp.bfloat16).reshape(normed.shape[0], EXPERTS, CAP, normed.shape[2])


def expert_hidden(arrived, gate_weight, up_weight):
    gate_proj = jnp.einsum(
        "besd,edf->besf", arrived, gate_weight, preferred_element_type=jnp.float32
    )
    up_proj = jnp.einsum("besd,edf->besf", arrived, up_weight, preferred_element_type=jnp.float32)
    return (jax.nn.silu(gate_proj) * up_proj).astype(jnp.bfloat16)


def mixer_half(
    mix_tokens, mix_gain, value_weight, inner_weight, outer_weight, conv_taps, mix_weight
):
    normed = rms_rows(mix_tokens, mix_gain)
    value_proj = jnp.dot(normed, value_weight, preferred_element_type=jnp.float32)
    inner_proj = jnp.dot(normed, inner_weight, preferred_element_type=jnp.float32)
    outer_proj = jnp.dot(normed, outer_weight, preferred_element_type=jnp.float32)
    gated_in = (inner_proj * value_proj).astype(jnp.bfloat16)
    earlier = from_behind(gated_in[gated_in.shape[0] - (TAPS - 1) :], "ep", 1)
    padded = jnp.concatenate([earlier, gated_in], axis=0).astype(jnp.float32)
    seq_rows = gated_in.shape[0]
    mixed_conv = conv_taps[0] * padded[0:seq_rows]
    for tap_index in range(1, TAPS):
        mixed_conv = mixed_conv + conv_taps[tap_index] * padded[tap_index : tap_index + seq_rows]
    conv_out = (outer_proj * mixed_conv).astype(jnp.bfloat16)
    summed = lax.psum_scatter(
        jnp.dot(conv_out, mix_weight, preferred_element_type=jnp.float32),
        "tp",
        scatter_dimension=0,
        tiled=True,
    )
    return summed.astype(jnp.bfloat16)


def local(
    mix_tokens,
    mix_gain,
    value_weight,
    inner_weight,
    outer_weight,
    conv_taps,
    mix_weight,
    moe_tokens,
    moe_gain,
    router_group,
    router_expert,
    expert_routes,
    gate_weight,
    up_weight,
    down_weight,
):
    mixer_out = mixer_half(
        mix_tokens, mix_gain, value_weight, inner_weight, outer_weight, conv_taps, mix_weight
    )
    tp_index = lax.axis_index("tp")
    model_width = moe_tokens.shape[1]
    own_routes = lax.dynamic_slice_in_dim(expert_routes, tp_index * MOE_SHARE, MOE_SHARE, 0)
    own_tokens = lax.dynamic_slice_in_dim(moe_tokens, tp_index * MOE_SHARE, MOE_SHARE, 0)
    own_normed = rms_rows(own_tokens, moe_gain)
    placed = dispatch_rows(own_normed[None], own_routes[None])[0]
    arrived = lax.all_to_all(placed, "ep", split_axis=0, concat_axis=1, tiled=True)
    hidden = expert_hidden(
        lax.all_gather(arrived[None], "tp", axis=0, tiled=True), gate_weight, up_weight
    )
    local_experts = hidden.shape[1]
    slot_count = hidden.shape[2]
    per_block = local_experts * slot_count
    partial_value = jnp.einsum(
        "besf,efd->besd", hidden, down_weight, preferred_element_type=jnp.float32
    )
    summed = lax.psum_scatter(
        partial_value.reshape(per_block * lax.axis_size("tp"), model_width),
        "tp",
        scatter_dimension=0,
        tiled=True,
    )
    results = summed.astype(jnp.bfloat16).reshape(
        local_experts, slot_count // CAP, CAP, model_width
    )
    returned = lax.all_to_all(results, "ep", split_axis=1, concat_axis=0, tiled=True).reshape(
        EXPERTS * CAP, model_width
    )
    weights = route_weights(own_normed, own_routes, router_group, router_expert)
    own_slots = own_routes * CAP + block_ranks(own_routes[None])[0]
    picked = jnp.take(returned, own_slots, axis=0).astype(jnp.float32)
    expert_out = jnp.sum(weights[:, :, None] * picked, axis=1).astype(jnp.bfloat16)
    return (mixer_out, expert_out)


def solution(mesh):
    return jax.shard_map(
        local,
        mesh=mesh,
        in_specs=(
            P("ep", None),
            P(),
            P(None, "tp"),
            P(None, "tp"),
            P(None, "tp"),
            P(None, "tp"),
            P("tp", None),
            P("ep", None),
            P(),
            P(),
            P(),
            P("ep", None),
            P("ep", None, "tp"),
            P("ep", None, "tp"),
            P("ep", "tp", None),
        ),
        out_specs=(P(("ep", "tp"), None), P(("ep", "tp"), None)),
        check_vma=False,
    )
```

profile of v0, /device:TPU:2, one launch (start us, length us, event | category | flops | bytes accessed | tf_op | source)
XLA Modules:
  0.0 281.7 jit_solution(8360812834643250856)
XLA Ops:
  7.2 0.0 all-gather.2.cloned.1.call-start
  7.2 0.8 constant_dynamic-slice_fusion
  8.1 0.1 copy.25
  8.1 0.1 eq.90
  8.2 0.1 fusion.48
  8.3 0.1 reduce_window_sum.12
  8.4 0.2 select_reduce_fusion
  8.6 0.1 squeeze_reshape.6
  8.6 0.1 copy.26
  8.7 0.8 compare_and_fusion
  9.5 0.1 convert_reduce_fusion
  9.6 1.0 fusion.37
  10.6 1.3 convolution_convert_fusion
  11.9 0.2 squeeze_reshape.7
  12.1 17.4 %all_to_all.8 = bf16[16,4,4096]{2,1,0:T(4,128)(2,1)S(1)} all-to-all(bf16[16,4,4096]{2,1,0:T(4,128)(2,1)S(1)} %squeeze_reshape.7), channel_id=1, replica_groups=mesh['ep'=16,'tp'=16] {'ep'}, dimensions={0} | all-to-all | bytes 1048576 | tf_op jit(solution)/shard_map/all_to_all | solution.py:120
  29.5 0.9 broadcast_in_dim.12
  30.5 0.0 all-gather.2.cloned.1.call-update
  30.5 0.0 reduce-scatter.5.cloned.1.call-start
  30.5 55.9 %all-gather.2.cloned.1.call-done = bf16[16,1,64,4096]{3,2,1,0:T(8,128)(2,1)} async-done(((bf16[1,1,64,4096]{3,2,1,0:T(8,128)(2,1)}), bf16[16,1,64,4096]{3,2,1,0:T(8,128)(2,1)}) %all-gather.2.cloned.1.call-update) | async-done | bytes 8388624 | tf_op jit(solution)/shard_map/all_gather | solution.py:122
  86.5 5.9 %fusion.7 = f32[16,1,64,128]{3,2,0,1:T(8,128)S(1)} fusion(bf16[16,1,64,4096]{3,2,1,0:T(8,128)(2,1)} %all-gather.2.cloned.1.call-done, bf16[1,4096,128]{2,1,0:T(8,128)(2,1)} %param.27), kind=kOutput, calls=%fused_computation.11 | convolution fusion | flops 1073741824 | bytes 9961472 | tf_op jit(solution)/shard_map/besd,edf->besf/dot_general | solution.py:63
  92.4 14.4 %fusion.23 = f32[16,64,4096]{2,1,0:T(8,128)} fusion(bf16[16,1,64,4096]{3,2,1,0:T(8,128)(2,1)} %all-gather.2.cloned.1.call-done, bf16[1,128,4096]{2,1,0:T(8,128)(2,1)S(1)} %copy-done, bf16[1,4096,128]{2,1,0:T(8,128)(2,1)S(1)} %copy-done.2, f32[16,1,64,128]{3,2,0,1:T(8,128)S(1)} %fusion.7), kind=kOutput, calls=%fused_computation.16 | convolution fusion | flops 2148270080 | bytes 27787264 | tf_op jit(solution)/shard_map/besf,efd->besd/dot_general | solution.py:127
  106.8 0.0 reduce-scatter.3.cloned.1.call-start
  106.9 1.5 copy-done.1
  108.4 0.5 fusion.4
  108.9 2.1 fusion.57
  111.0 0.9 fusion.26
  111.9 3.4 %collective-permute-start = (bf16[2,128]{1,0:T(2,128)(2,1)S(1)}, bf16[2,128]{1,0:T(2,128)(2,1)S(1)}, u32[]{:S(2)}, u32[]{:S(2)}) collective-permute-start(bf16[2,128]{1,0:T(2,128)(2,1)S(1)} %slice.34), channel_id=1, source_target_pairs={{0,16},{16,32},{32,48},{48,64},{64,80},{80,96},{96,112},{112,128},... | collective-permute-start | bytes 1544 | tf_op jit(solution)/shard_map/ppermute | solution.py:18
  115.3 2.1 collective-permute-done
  117.4 5.0 %fusion.27 = f32[256,4096]{1,0:T(8,128)} fusion(bf16[128,4096]{1,0:T(8,128)(2,1)} %param.21, bf16[4096,128]{1,0:T(8,128)(2,1)} %param.19, f32[258,128]{1,0:T(8,128)S(1)} %maximum_convert_fusion, f32[128]{0:T(128)S(1)} %get-tuple-element.7, f32[128]{0:T(128)S(1)} %get-tuple-element.8, f32[128]{0:T(128)S(1)} %get-tuple-element.6, ...), kind=kOutput, calls=%fused_computation.21 | convolution fusion | flops 541294592 | bytes 8800768 | tf_op jit(solution)/shard_map/dot_general | solution.py:86
  122.4 0.7 copy-done.4
  123.1 0.1 copy-done.8
  123.1 1.2 fusion.61
  124.3 1.1 fusion.53
  125.5 80.6 %reduce-scatter.5.cloned.1.call-done = f32[64,4096]{1,0:T(8,128)} async-done(((f32[1024,4096]{1,0:T(8,128)}), f32[64,4096]{1,0:T(8,128)}) %reduce-scatter.5.cloned.1.call-update) | async-done | bytes 1048592 | tf_op jit(solution)/shard_map/reduce_scatter | solution.py:130
  206.1 1.3 convert_element_type.92
  207.4 1.0 reshape.229
  208.4 7.3 %all-to-all-start.1 = ((bf16[1,16,4,4096]{3,2,0,1:T(4,128)(2,1)}), bf16[1,16,4,4096]{3,2,0,1:T(4,128)(2,1)S(1)}, u32[]{:S(2)}, u32[]{:S(2)}) async-start(bf16[1,16,4,4096]{3,2,0,1:T(4,128)(2,1)} %reshape.229), calls=%async_computation.3 | async-start | bytes 1048576 | tf_op jit(solution)/shard_map/all_to_all | solution.py:139
  215.6 0.2 select_reduce_fusion.1
  215.8 0.1 copy.28
  215.9 0.1 reshape.233
  216.0 0.1 copy.24
  216.1 0.1 copy.27
  216.2 54.8 %reduce-scatter.3.cloned.1.call-done = f32[16,4096]{1,0:T(8,128)} async-done(((f32[256,4096]{1,0:T(8,128)}), f32[16,4096]{1,0:T(8,128)}) %reduce-scatter.3.cloned.1.call-update) | async-done | bytes 262160 | tf_op jit(solution)/shard_map/reduce_scatter | solution.py:85
  271.0 1.6 convert_element_type.84
  272.7 0.1 reshape.230
  272.8 0.7 gather_fusion
  273.5 0.2 reshape.232
  273.7 1.5 multiply_reduce_fusion
  (29 shorter events, 0.2 us)
Async XLA Ops:
  7.2 85.2 %copy-start = (bf16[1,128,4096]{2,1,0:T(8,128)(2,1)S(1)}, bf16[1,128,4096]{2,1,0:T(8,128)(2,1)}, u32[]{:S(2)}) copy-start(bf16[1,128,4096]{2,1,0:T(8,128)(2,1)} %param.29) | copy-start | bytes 3145732
  7.2 79.3 %all-gather.2.cloned.1.call-start = ((), (), s32[]{:S(2)}) async-start(), calls=%async_computation.5 | async-start | bytes 8912896 | tf_op jit(solution)/shard_map/all_gather | solution.py:122
  30.5 61.9 %copy-start.2 = (bf16[1,4096,128]{2,1,0:T(8,128)(2,1)S(1)}, bf16[1,4096,128]{2,1,0:T(8,128)(2,1)}, u32[]{:S(2)}) copy-start(bf16[1,4096,128]{2,1,0:T(8,128)(2,1)} %param.28) | copy-start | bytes 3145732
  30.5 175.6 %reduce-scatter.5.cloned.1.call-start = ((), (), s32[]{:S(2)}) async-start(), calls=%async_computation.6 | async-start | bytes 17825792 | tf_op jit(solution)/shard_map/reduce_scatter | solution.py:130
  106.8 1.6 copy-start.1
  106.8 2.1 copy-start.3
  106.8 164.2 %reduce-scatter.3.cloned.1.call-start = ((), (), s32[]{:S(2)}) async-start(), calls=%async_computation.4 | async-start | bytes 4456448 | tf_op jit(solution)/shard_map/reduce_scatter | solution.py:85
  108.4 2.6 copy-start.6
  108.9 6.4 %copy-start.5 = (f32[3,128]{1,0:T(4,128)S(1)}, f32[3,128]{1,0:T(4,128)}, u32[]{:S(2)}) copy-start(f32[3,128]{1,0:T(4,128)} %param.20) | copy-start | bytes 4612
  111.9 5.5 %collective-permute-start = (bf16[2,128]{1,0:T(2,128)(2,1)S(1)}, bf16[2,128]{1,0:T(2,128)(2,1)S(1)}, u32[]{:S(2)}, u32[]{:S(2)}) collective-permute-start(bf16[2,128]{1,0:T(2,128)(2,1)S(1)} %slice.34), channel_id=1, source_target_pairs={{0,16},{16,32},{32,48},{48,64},{64,80},{80,96},{96,112},{112,128},... | collective-permute-start | bytes 1544 | tf_op jit(solution)/shard_map/ppermute | solution.py:18
  122.4 0.7 copy-start.4
  122.4 0.8 copy-start.8
  122.4 1.9 copy-start.7
  208.4 64.3 %all-to-all-start.1 = ((bf16[1,16,4,4096]{3,2,0,1:T(4,128)(2,1)}), bf16[1,16,4,4096]{3,2,0,1:T(4,128)(2,1)S(1)}, u32[]{:S(2)}, u32[]{:S(2)}) async-start(bf16[1,16,4,4096]{3,2,0,1:T(4,128)(2,1)} %reshape.229), calls=%async_computation.3 | async-start | bytes 1048576 | tf_op jit(solution)/shard_map/all_to_all | solution.py:139
Sparse Core Ops, SparseCore 0:
  30.6 55.8 all-gather.1
  107.0 99.0 reduce-scatter.4
  208.6 62.3 reduce-scatter.2
where the time goes:
time: 282 us
  waiting for transfers between devices  193 us (68%)
  matrix products  31.8 us (11%)
  blocking collectives  17.4 us (6%)
  between operations  14 us (5%)
  starting transfers between devices  10.8 us (4%)
  other arithmetic  7.33 us (3%)
  local copies, waits for them, and re-layouts  6.92 us (2%)
    reduce_scatter x1, waiting for transfers between devices, local(): lax.psum_scatter(partial_value.reshape(per_block * lax.axis_size('tp'), m...  80.6 us
    all_gather x1, waiting for transfers between devices, local(): lax.all_gather(arrived[None], 'tp', axis=0, tiled=True)  55.9 us
    reduce_scatter x1, waiting for transfers between devices, mixer_half(): lax.psum_scatter(jnp.dot(conv_out, mix_weight, preferred_element_type=jnp...  54.8 us
    all_to_all x1, blocking collectives, local(): lax.all_to_all(placed, 'ep', split_axis=0, concat_axis=1, tiled=True)  17.4 us
    dot_general x1, matrix products, local(): jnp.einsum('besf,efd->besd', hidden, down_weight, preferred_element_type=...  14.4 us
    all_to_all x1, starting transfers between devices, local(): lax.all_to_all(results, 'ep', split_axis=1, concat_axis=0, tiled=True)  7.27 us
    dot_general x1, matrix products, expert_hidden(): jnp.einsum('besd,edf->besf', arrived, gate_weight, preferred_element_type...  5.93 us
  transfers between devices with their start and end apart: 5, of which 4 were waited for; matrix products, arithmetic and copies ran while one was open for 5% of the time, Pallas kernels for 0%

commit v1 on v0

--- a/solution.py
+++ b/solution.py
@@ -10,6 +10,13 @@
 MOE_SHARE = 16
 EPG = 4
 CAP = 4
+
+
+def outputs_search(piece_in, group_axis, dimension_no):
+    part_next = lax.axis_size(group_axis)
+    new = jnp.concatenate([piece_in] * part_next, axis=dimension_no)
+    part_now = lax.all_to_all(new, group_axis, dimension_no, dimension_no, tiled=True)
+    return part_now
 
 
 def from_behind(value, axis, steps):
@@ -118,9 +125,7 @@
     own_normed = rms_rows(own_tokens, moe_gain)
     placed = dispatch_rows(own_normed[None], own_routes[None])[0]
     arrived = lax.all_to_all(placed, "ep", split_axis=0, concat_axis=1, tiled=True)
-    hidden = expert_hidden(
-        lax.all_gather(arrived[None], "tp", axis=0, tiled=True), gate_weight, up_weight
-    )
+    hidden = expert_hidden(outputs_search(arrived[None], "tp", 0), gate_weight, up_weight)
     local_experts = hidden.shape[1]
     slot_count = hidden.shape[2]
     per_block = local_experts * slot_count

time: 282 us -> 417 us (1.48)
  blocking collectives: 17.4 us -> 210 us
  waiting for transfers between devices: 193 us -> 136 us
    all_to_all x0 -> x1, blocking collectives: none -> 193 us  [outputs_search(): lax.all_to_all(new, group_axis, dimension_no, dimension_no, tiled=True)]
    all_gather x1 -> x0, waiting for transfers between devices: 55.9 us -> none  [local(): lax.all_gather(arrived[None], 'tp', axis=0, tiled=True)]
  transfers between devices with their start and end apart: 5 -> 4, of which waited for: 4 -> 3; matrix products, arithmetic and copies ran while one was open for 5% -> 4% of each run, Pallas kernels for 0% -> 0%
where the time goes in v1:
time: 417 us; the launch traced here: 416 us
  blocking collectives  210 us (50%)
  waiting for transfers between devices  136 us (33%)
  matrix products  28.1 us (7%)
  between operations  14.3 us (3%)
  local copies, waits for them, and re-layouts  10.4 us (2%)
  starting transfers between devices  9.45 us (2%)
  other arithmetic  7.33 us (2%)
    all_to_all x1, blocking collectives, outputs_search(): lax.all_to_all(new, group_axis, dimension_no, dimension_no, tiled=True)  193 us
    reduce_scatter x1, waiting for transfers between devices, local(): lax.psum_scatter(partial_value.reshape(per_block * lax.axis_size('tp'), m...  77.8 us
    reduce_scatter x1, waiting for transfers between devices, mixer_half(): lax.psum_scatter(jnp.dot(conv_out, mix_weight, preferred_element_type=jnp...  54.8 us
    all_to_all x1, blocking collectives, local(): lax.all_to_all(placed, 'ep', split_axis=0, concat_axis=1, tiled=True)  17.4 us
    dot_general x1, matrix products, local(): jnp.einsum('besf,efd->besd', hidden, down_weight, preferred_element_type=...  14.4 us
  transfers between devices with their start and end apart: 4, of which 3 were waited for; matrix products, arithmetic and copies ran while one was open for 4% of the time, Pallas kernels for 0%

profile of v1, /device:TPU:2, one launch (start us, length us, event | category | flops | bytes accessed | tf_op | source)
XLA Modules:
  0.0 415.9 jit_solution(16299632416693376285)
XLA Ops:
  7.2 0.0 reduce-scatter.5.cloned.1.call-start
  7.2 0.8 constant_dynamic-slice_fusion
  8.1 0.1 copy.25
  8.1 0.1 eq.90
  8.2 0.1 fusion.48
  8.3 0.1 reduce_window_sum.12
  8.4 0.2 select_reduce_fusion
  8.6 0.1 squeeze_reshape.6
  8.6 0.1 copy.26
  8.7 0.8 compare_and_fusion
  9.5 0.1 convert_reduce_fusion
  9.6 1.0 fusion.37
  10.6 1.3 convolution_convert_fusion
  11.9 0.2 squeeze_reshape.7
  12.1 17.4 %all_to_all.23 = bf16[16,4,4096]{2,1,0:T(4,128)(2,1)S(1)} all-to-all(bf16[16,4,4096]{2,1,0:T(4,128)(2,1)S(1)} %squeeze_reshape.7), channel_id=1, replica_groups=mesh['ep'=16,'tp'=16] {'ep'}, dimensions={0} | all-to-all | bytes 1048576 | tf_op jit(solution)/shard_map/all_to_all | solution.py:127
  29.5 0.1 broadcast_in_dim.12
  29.7 1.0 concatenate.7
  30.7 193.0 %all_to_all.24 = bf16[16,1,64,4096]{3,2,1,0:T(8,128)(2,1)S(1)} all-to-all(bf16[16,1,64,4096]{3,2,1,0:T(8,128)(2,1)S(1)} %concatenate.7), channel_id=1, replica_groups=mesh['ep'=16,'tp'=16] {'tp'}, dimensions={0} | all-to-all | bytes 16777216 | tf_op jit(solution)/shard_map/all_to_all | solution.py:18
  223.7 3.2 copy-done.1
  226.9 2.3 fusion.7
  229.3 14.4 %fusion.23 = f32[16,64,4096]{2,1,0:T(8,128)} fusion(bf16[16,1,64,4096]{3,2,1,0:T(8,128)(2,1)} %copy-done.1, bf16[1,128,4096]{2,1,0:T(8,128)(2,1)S(1)} %copy-done, bf16[1,4096,128]{2,1,0:T(8,128)(2,1)S(1)} %copy-done.3, f32[16,1,64,128]{3,2,0,1:T(8,128)S(1)} %fusion.7), kind=kOutput, calls=%fused_computation.16 | convolution fusion | flops 2148270080 | bytes 27787264 | tf_op jit(solution)/shard_map/besf,efd->besd/dot_general | solution.py:132
  243.7 0.0 reduce-scatter.3.cloned.1.call-start
  243.7 1.5 copy-done.2
  245.2 0.5 fusion.4
  245.8 2.1 fusion.57
  247.8 0.9 fusion.26
  248.7 2.1 collective-permute-start
  250.9 3.3 collective-permute-done
  254.2 4.9 %fusion.27 = f32[256,4096]{1,0:T(8,128)} fusion(bf16[128,4096]{1,0:T(8,128)(2,1)} %param.21, bf16[4096,128]{1,0:T(8,128)(2,1)} %param.19, f32[258,128]{1,0:T(8,128)S(1)} %maximum_convert_fusion, f32[128]{0:T(128)S(1)} %get-tuple-element.7, f32[128]{0:T(128)S(1)} %get-tuple-element.8, f32[128]{0:T(128)S(1)} %get-tuple-element.6, ...), kind=kOutput, calls=%fused_computation.21 | convolution fusion | flops 541294592 | bytes 8800768 | tf_op jit(solution)/shard_map/dot_general | solution.py:93
  259.2 0.7 copy-done.5
  259.8 0.1 copy-done.10
  259.9 1.2 fusion.61
  261.1 1.1 fusion.53
  262.2 77.8 %reduce-scatter.5.cloned.1.call-done = f32[64,4096]{1,0:T(8,128)} async-done(((f32[1024,4096]{1,0:T(8,128)}), f32[64,4096]{1,0:T(8,128)}) %reduce-scatter.5.cloned.1.call-update) | async-done | bytes 1048592 | tf_op jit(solution)/shard_map/reduce_scatter | solution.py:135
  340.1 1.3 convert_element_type.92
  341.3 1.0 reshape.233
  342.3 7.3 %all-to-all-start.2 = ((bf16[1,16,4,4096]{3,2,0,1:T(4,128)(2,1)}), bf16[1,16,4,4096]{3,2,0,1:T(4,128)(2,1)S(1)}, u32[]{:S(2)}, u32[]{:S(2)}) async-start(bf16[1,16,4,4096]{3,2,0,1:T(4,128)(2,1)} %reshape.233), calls=%async_computation.4 | async-start | bytes 1048576 | tf_op jit(solution)/shard_map/all_to_all | solution.py:144
  349.6 0.2 select_reduce_fusion.1
  349.7 0.1 copy.28
  349.8 0.1 reshape.237
  350.0 0.1 copy.24
  350.0 0.1 copy.27
  350.2 54.8 %reduce-scatter.3.cloned.1.call-done = f32[16,4096]{1,0:T(8,128)} async-done(((f32[256,4096]{1,0:T(8,128)}), f32[16,4096]{1,0:T(8,128)}) %reduce-scatter.3.cloned.1.call-update) | async-done | bytes 262160 | tf_op jit(solution)/shard_map/reduce_scatter | solution.py:92
  405.0 1.6 convert_element_type.84
  406.6 0.1 reshape.234
  406.7 0.7 gather_fusion
  407.4 0.2 reshape.236
  407.6 1.5 multiply_reduce_fusion
  (32 shorter events, 0.2 us)
Async XLA Ops:
  7.2 222.1 %copy-start = (bf16[1,128,4096]{2,1,0:T(8,128)(2,1)S(1)}, bf16[1,128,4096]{2,1,0:T(8,128)(2,1)}, u32[]{:S(2)}) copy-start(bf16[1,128,4096]{2,1,0:T(8,128)(2,1)} %param.29) | copy-start | bytes 3145732
  7.2 332.9 %reduce-scatter.5.cloned.1.call-start = ((), (), s32[]{:S(2)}) async-start(), calls=%async_computation.6 | async-start | bytes 17825792 | tf_op jit(solution)/shard_map/reduce_scatter | solution.py:135
  30.7 196.2 %copy-start.7 = (bf16[1,4096,128]{2,1,0:T(8,128)(2,1)S(1)}, bf16[1,4096,128]{2,1,0:T(8,128)(2,1)}, u32[]{:S(2)}) copy-start(bf16[1,4096,128]{2,1,0:T(8,128)(2,1)} %param.27) | copy-start | bytes 3145732
  223.7 3.2 copy-start.1
  226.9 2.3 copy-start.3
  243.7 1.6 copy-start.2
  243.7 2.1 copy-start.4
  243.7 161.3 %reduce-scatter.3.cloned.1.call-start = ((), (), s32[]{:S(2)}) async-start(), calls=%async_computation.5 | async-start | bytes 4456448 | tf_op jit(solution)/shard_map/reduce_scatter | solution.py:92
  245.2 2.6 copy-start.8
  245.8 5.1 %copy-start.6 = (f32[3,128]{1,0:T(4,128)S(1)}, f32[3,128]{1,0:T(4,128)}, u32[]{:S(2)}) copy-start(f32[3,128]{1,0:T(4,128)} %param.20) | copy-start | bytes 4612
  248.7 5.5 %collective-permute-start = (bf16[2,128]{1,0:T(2,128)(2,1)S(1)}, bf16[2,128]{1,0:T(2,128)(2,1)S(1)}, u32[]{:S(2)}, u32[]{:S(2)}) collective-permute-start(bf16[2,128]{1,0:T(2,128)(2,1)S(1)} %slice.34), channel_id=1, source_target_pairs={{0,16},{16,32},{32,48},{48,64},{64,80},{80,96},{96,112},{112,128},... | collective-permute-start | bytes 1544 | tf_op jit(solution)/shard_map/ppermute | solution.py:25
  259.1 0.7 copy-start.5
  259.1 0.8 copy-start.10
  259.1 1.9 copy-start.9
  342.3 64.3 %all-to-all-start.2 = ((bf16[1,16,4,4096]{3,2,0,1:T(4,128)(2,1)}), bf16[1,16,4,4096]{3,2,0,1:T(4,128)(2,1)S(1)}, u32[]{:S(2)}, u32[]{:S(2)}) async-start(bf16[1,16,4,4096]{3,2,0,1:T(4,128)(2,1)} %reshape.233), calls=%async_computation.4 | async-start | bytes 1048576 | tf_op jit(solution)/shard_map/all_to_all | solution.py:144
Sparse Core Ops, SparseCore 0:
  243.8 96.2 reduce-scatter.4
  342.6 62.3 reduce-scatter.2
